TPU v7x, 32 devices: a whole 2x2x4 slice. The times are simulated.
32 devices in a mesh: sp: 16 (over z, y, core), tp: 2 (over x).
Axes of the slice: x: 2, y: 2, z: 4, core: 2. Of those that a mesh axis runs over, the one named last changes fastest.
Arguments:
- tokens: bfloat16 [1536, 2048], P('sp'), may hold values from -2500 to 2500
- query_down: bfloat16 [2048, 512], replicated, may hold values from -0.125 to 0.125
- latent_down: bfloat16 [2048, 512], replicated, may hold values from -0.125 to 0.125
- rope_down: bfloat16 [2048, 64], replicated, may hold values from -0.125 to 0.125
- query_gain: float32 [512], replicated, may hold values from 0.1 to 1.9
- latent_gain: float32 [512], replicated, may hold values from 0.1 to 1.9
- query_up: bfloat16 [512, 512], P(None, 'tp'), may hold values from -0.25 to 0.25
- query_rope: bfloat16 [512, 256], P(None, 'tp'), may hold values from -0.25 to 0.25
- key_up: bfloat16 [512, 512], P(None, 'tp'), may hold values from -0.25 to 0.25
- value_up: bfloat16 [512, 512], P(None, 'tp'), may hold values from -0.25 to 0.25
- out_proj: bfloat16 [512, 2048], replicated, may hold values from -0.25 to 0.25
- out_gain: float32 [2048], replicated, may hold values from 0.1 to 1.9
Outputs:
- mixed: bfloat16 [1536, 2048], P('sp')
All inputs are finite; a program needn't handle non-finite values.
Results may differ from a plain program's by a relative error of at most 0.035.
Values may be sent and summed in bfloat16 or wider, within the bound.
A program may use at most 64 MiB of HBM per device.

v0:
```python
import jax
import jax.numpy as jnp
from jax import lax
from jax.sharding import PartitionSpec as P

HEADS = 4
NOPE = 128
ROPE = 64
VDIM = 128
SEQS = 8


EPS = 1e-06
THETA = 10000.0


def as_sent(value):
    return jax.tree.map(lambda a: a.astype(jnp.bfloat16) if a.dtype == jnp.float32 else a, value)


def swapped(value, axis, apart):
    mask = 2**apart
    pairs = [(source, source ^ mask) for source in range(lax.axis_size(axis))]
    return lax.ppermute(value, axis, pairs)


def normalize(rows, gain):
    mean_sq = jnp.mean(rows * rows, axis=-1, keepdims=True)
    return rows * lax.rsqrt(mean_sq + EPS) * gain


def angles(positions, width):
    half = width // 2
    freq = THETA ** (-jnp.arange(half, dtype=jnp.float32) / half)
    angle = positions[:, None] * freq[None, :]
    return (jnp.cos(angle), jnp.sin(angle))


def rotate(rows, cosine, sine):
    half = rows.shape[-1] // 2
    first = rows[..., :half]
    second = rows[..., half:]
    return jnp.concatenate(
        [first * cosine - second * sine, first * sine + second * cosine], axis=-1
    )


def join_parts(holding, incoming):
    return tuple(
        (
            jnp.concatenate([held_part, new_part], axis=0)
            for held_part, new_part in zip(holding, incoming)
        )
    )


def on_device(
    tokens,
    query_down,
    latent_down,
    rope_down,
    query_gain,
    latent_gain,
    query_up,
    query_rope,
    key_up,
    value_up,
    out_proj,
    out_gain,
):
    tp_size = lax.axis_size("tp")
    group_size = lax.axis_size("sp") // SEQS
    sections = group_size.bit_length() - 1
    heads_dev = HEADS // tp_size
    rows_dev = tokens.shape[0]
    scale = (NOPE + ROPE) ** (-0.5)
    first_row = lax.axis_index("sp") % group_size * rows_dev
    positions = (first_row + jnp.arange(rows_dev, dtype=jnp.int32)).astype(jnp.float32)
    cosine, sine = angles(positions, ROPE)
    q_latent = normalize(
        jnp.dot(tokens, query_down, preferred_element_type=jnp.float32), query_gain
    ).astype(jnp.bfloat16)
    kv_latent = normalize(
        jnp.dot(tokens, latent_down, preferred_element_type=jnp.float32), latent_gain
    ).astype(jnp.bfloat16)
    rope_key = rotate(
        jnp.dot(tokens, rope_down, preferred_element_type=jnp.float32), cosine, sine
    ).astype(jnp.bfloat16)
    q_nope = jnp.dot(q_latent, query_up, preferred_element_type=jnp.float32).astype(jnp.bfloat16)
    q_nope = q_nope.reshape(rows_dev, heads_dev, NOPE)
    q_rot = rotate(
        jnp.dot(q_latent, query_rope, preferred_element_type=jnp.float32).reshape(
            rows_dev, heads_dev, ROPE
        ),
        cosine[:, None, :],
        sine[:, None, :],
    ).astype(jnp.bfloat16)

    def expand(latent):
        keys = jnp.dot(latent, key_up, preferred_element_type=jnp.float32).astype(jnp.bfloat16)
        values = jnp.dot(latent, value_up, preferred_element_type=jnp.float32).astype(jnp.bfloat16)
        return (keys, values)

    def attend(carry, keys, values, rope_piece):
        highest, total, weighted = carry
        count = keys.shape[0]
        keys = keys.reshape(count, heads_dev, NOPE)
        values = values.reshape(count, heads_dev, VDIM)
        scores = (
            jnp.einsum("qhd,khd->hqk", q_nope, keys, preferred_element_type=jnp.float32)
            + jnp.einsum("qhr,kr->hqk", q_rot, rope_piece, preferred_element_type=jnp.float32)
        ) * scale
        new_high = jnp.maximum(highest, jnp.max(scores, axis=-1))
        factor = jnp.exp(highest - new_high)
        expd = jnp.exp(scores - new_high[..., None])
        total = total * factor + jnp.sum(expd, axis=-1)
        weighted = weighted * factor[..., None] + jnp.einsum(
            "hqk,khv->hqv", expd.astype(jnp.bfloat16), values, preferred_element_type=jnp.float32
        )
        return (new_high, total, weighted)

    carry = (
        jnp.full((heads_dev, rows_dev), -jnp.inf, jnp.float32),
        jnp.zeros((heads_dev, rows_dev), jnp.float32),
        jnp.zeros((heads_dev, rows_dev, VDIM), jnp.float32),
    )
    holding = (kv_latent, rope_key)
    own_keys, own_values = expand(kv_latent)
    carry = attend(carry, own_keys, own_values, rope_key)
    for level in range(sections):
        incoming = jax.tree.map(
            lambda part, own: part.astype(own.dtype),
            swapped(as_sent(holding), "sp", level),
            holding,
        )
        far_keys, far_values = expand(incoming[0])
        carry = attend(carry, far_keys, far_values, incoming[1])
        if level + 1 < sections:
            holding = join_parts(holding, incoming)
    highest, total, weighted = carry
    attn = (weighted / total[..., None]).astype(jnp.bfloat16)
    attn_rows = jnp.transpose(attn, (1, 0, 2)).reshape(rows_dev, heads_dev * VDIM)
    projected = jnp.dot(
        lax.all_gather(attn_rows, "tp", axis=1, tiled=True),
        out_proj,
        preferred_element_type=jnp.float32,
    )
    return normalize(projected, out_gain).astype(jnp.bfloat16)


def solution(mesh):
    in_specs = (
        P("sp", None),
        P(),
        P(),
        P(),
        P(),
        P(),
        P(None, "tp"),
        P(None, "tp"),
        P(None, "tp"),
        P(None, "tp"),
        P(),
        P(),
    )
    out_specs = P("sp", None)
    return jax.shard_map(
        on_device, mesh=mesh, in_specs=in_specs, out_specs=out_specs, check_vma=False
    )
```

profile of v0, /device:TPU:0, one launch (start us, length us, event | category | flops | bytes accessed | tf_op | source)
XLA Modules:
  0.0 15.2 jit_solution(14453447970086637557)
XLA Ops:
  0.0 0.0 copy-start
  0.0 0.0 copy-start.1
  0.0 0.0 copy-start.9
  0.0 0.0 copy-start.2
  0.1 1.5 %fusion.49 = f32[96,64]{0,1:T(8,128)S(1)} fusion(bf16[96,2048]{1,0:T(8,128)(2,1)} %param.12, bf16[2048,64]{0,1:T(8,128)(2,1)} %param.15), kind=kOutput, calls=%fused_computation.81 | convolution fusion | flops 25165824 | bytes 679936 | tf_op jit(solution)/shard_map/dot_general | solution.py:87
  1.5 0.1 subtract_convert_fusion.1
  1.7 0.6 %collective-permute-start.1 = (bf16[96,64]{0,1:T(8,128)(2,1)S(1)}, bf16[96,64]{0,1:T(8,128)(2,1)S(1)}, u32[]{:S(2)}, u32[]{:S(2)}) collective-permute-start(bf16[96,64]{0,1:T(8,128)(2,1)S(1)} %pad_maximum_fusion.3), channel_id=1, source_target_pairs={{0,2},{2,0},{4,6},{6,4},{8,10},{10,8},{12,14},{14,12},{16,18},{18,... | collective-permute-start | bytes 36872 | tf_op jit(solution)/shard_map/ppermute | solution.py:24
  2.3 2.3 %multiply_reduce_fusion.1 = (f32[96]{0:T(128)S(1)}, f32[96,512]{1,0:T(8,128)S(1)}) fusion(bf16[96,2048]{1,0:T(8,128)(2,1)} %param.12, bf16[2048,512]{1,0:T(8,128)(2,1)} %param.14), kind=kOutput, calls=%fused_computation.27 | convolution fusion | flops 201424800 | bytes 2687360 | tf_op jit(solution)/shard_map/dot_general | solution.py:84
  4.6 0.0 copy-start.5
  4.6 0.0 copy-start.8
  4.6 0.0 copy-start.6
  4.6 0.0 copy-start.4
  4.6 0.0 copy-done.9
  4.7 0.0 copy-start.3
  4.7 0.1 multiply_convert_fusion.1
  4.8 0.1 collective-permute-start
  4.8 0.0 copy-done.1
  4.8 0.0 copy-done.2
  4.9 0.6 %multiply_reduce_fusion.2 = (f32[96]{0:T(128)S(1)}, f32[96,512]{1,0:T(8,128)S(1)}) fusion(bf16[96,2048]{1,0:T(8,128)(2,1)S(1)} %copy-done.1, bf16[2048,512]{1,0:T(8,128)(2,1)S(1)} %copy-done.2), kind=kOutput, calls=%fused_computation.29 | convolution fusion | flops 201424800 | bytes 2687360 | tf_op jit(solution)/shard_map/dot_general | solution.py:81
  5.4 0.1 copy-done.5
  5.5 0.0 copy-done.8
  5.5 0.2 %fusion.9 = bf16[12,2,8,128]{3,2,1,0:T(8,128)(2,1)S(1)} fusion(bf16[512,256]{1,0:T(8,128)(2,1)S(1)} %copy-done.5, f32[96,512]{1,0:T(8,128)S(1)} %get-tuple-element.17, f32[512]{0:T(512)S(1)} %copy-done.8, f32[96]{0:T(128)S(1)} %add_rsqrt_fusion.2), kind=kOutput, calls=%fused_computation.18 | convolution fusion | flops 25337856 | bytes 510336 | tf_op jit(solution)/shard_map/dot_general | solution.py:89
  5.8 0.0 copy-done.6
  5.8 0.3 %fusion.45 = f32[96,128]{0,1:T(8,128)S(1)} fusion(bf16[512,128]{1,0:T(8,128)(2,1)S(1)} %copy-done.6, f32[96,512]{1,0:T(8,128)S(1)} %get-tuple-element.17, f32[512]{0:T(512)S(1)} %copy-done.8, f32[96]{0:T(128)S(1)} %add_rsqrt_fusion.2), kind=kOutput, calls=%fused_computation.78 | convolution fusion | flops 12730368 | bytes 379264 | tf_op jit(solution)/shard_map/dot_general | solution.py:92
  6.0 0.0 copy-done.4
  6.1 0.2 %fusion.11 = bf16[12,2,8,128]{3,2,1,0:T(8,128)(2,1)S(1)} fusion(bf16[96,512]{1,0:T(8,128)(2,1)S(1)} %multiply_convert_fusion.1, bf16[512,256]{1,0:T(8,128)(2,1)S(1)} %copy-done.4), kind=kOutput, calls=%fused_computation.20 | convolution fusion | flops 25190400 | bytes 409600 | tf_op jit(solution)/shard_map/dot_general | solution.py:101
  6.2 0.0 copy-done.3
  6.3 0.2 %fusion.10 = bf16[12,2,8,128]{3,2,1,0:T(8,128)(2,1)S(1)} fusion(bf16[96,512]{1,0:T(8,128)(2,1)S(1)} %multiply_convert_fusion.1, bf16[512,256]{1,0:T(8,128)(2,1)S(1)} %copy-done.3), kind=kOutput, calls=%fused_computation.19 | convolution fusion | flops 25190400 | bytes 409600 | tf_op jit(solution)/shard_map/dot_general | solution.py:100
  6.4 0.1 fusion.28
  6.6 0.2 %fusion.47 = (f32[2,96]{1,0:T(2,128)S(1)}, f32[2,96,96]{1,2,0:T(8,128)S(1)}) fusion(f32[2,96,96]{1,2,0:T(8,128)S(1)} %fusion.28, bf16[96,2,32]{0,2,1:T(8,128)(2,1)S(1)} %get-tuple-element.8, bf16[96,2,32]{0,2,1:T(8,128)(2,1)S(1)} %get-tuple-element.7, bf16[96,32]{0,1:T(8,128)(2,1)S(1)} %get-tuple-element.10, bf16[96,32]{0,1:T(8,128)(2,1)S(1)} %get-tuple-element.9), kind=kOutput, calls=%fused_computation.79 | convolution fusion | flops 2488128 | bytes 185088 | tf_op jit(solution)/shard_map/qhr,kr->hqk/dot_general | solution.py:111
  6.9 0.0 collective-permute-done
  6.9 0.2 %fusion.12 = bf16[12,2,8,128]{3,2,1,0:T(8,128)(2,1)S(1)} fusion(bf16[96,512]{1,0:T(8,128)(2,1)S(1)} %collective-permute-done, bf16[512,256]{1,0:T(8,128)(2,1)S(1)} %copy-done.3), kind=kOutput, calls=%fused_computation.21 | convolution fusion | flops 25190400 | bytes 409600 | tf_op jit(solution)/shard_map/dot_general | solution.py:100
  7.1 0.1 fusion.23
  7.2 0.0 collective-permute-done.1
  7.2 0.2 %fusion.48 = (f32[2,96]{1,0:T(2,128)S(1)}, f32[2,96,96]{1,2,0:T(8,128)S(1)}) fusion(f32[2,96,96]{1,2,0:T(8,128)S(1)} %fusion.23, bf16[96,2,32]{0,2,1:T(8,128)(2,1)S(1)} %get-tuple-element.8, bf16[96,2,32]{0,2,1:T(8,128)(2,1)S(1)} %get-tuple-element.7, bf16[96,64]{0,1:T(8,128)(2,1)S(1)} %collective-permute-done.1), kind=kOutput, calls=%fused_computation.80 | convolution fusion | flops 2463552 | bytes 185088 | tf_op jit(solution)/shard_map/qhr,kr->hqk/dot_general | solution.py:111
  7.5 0.2 %fusion.5 = f32[96,2,128]{2,0,1:T(8,128)S(1)} fusion(f32[2,96,96]{1,2,0:T(8,128)S(1)} %get-tuple-element.19, bf16[12,2,8,128]{3,2,1,0:T(8,128)(2,1)S(1)} %fusion.11, f32[96,2]{0,1:T(2,128)S(1)} %get-tuple-element.6, f32[2,96]{1,0:T(2,128)S(1)} %get-tuple-element.18, f32[96,2]{0,1:T(2,128)S(1)} %get-tuple-element.11), kind=kOutput, calls=%fused_computation.8 | convolution fusion | flops 4804608 | bytes 223488 | tf_op jit(solution)/shard_map/hqk,khv->hqv/dot_general | solution.py:117
  7.7 0.0 copy-start.7
  7.7 0.2 %fusion.13 = bf16[12,2,8,128]{3,2,1,0:T(8,128)(2,1)S(1)} fusion(bf16[96,512]{1,0:T(8,128)(2,1)S(1)} %collective-permute-done, bf16[512,256]{1,0:T(8,128)(2,1)S(1)} %copy-done.4), kind=kOutput, calls=%fused_computation.22 | convolution fusion | flops 25190400 | bytes 409600 | tf_op jit(solution)/shard_map/dot_general | solution.py:101
  7.9 0.2 %fusion.14 = bf16[2,12,8,128]{3,2,1,0:T(8,128)(2,1)S(1)} fusion(f32[96,2,128]{2,0,1:T(8,128)S(1)} %fusion.5, f32[2,96,96]{1,2,0:T(8,128)S(1)} %get-tuple-element.21, bf16[12,2,8,128]{3,2,1,0:T(8,128)(2,1)S(1)} %fusion.13, f32[96,2]{0,1:T(2,128)S(1)} %get-tuple-element.5, f32[2,96]{1,0:T(2,128)S(1)} %max.18), kind=kOutput, calls=%fused_computation.23 | convolution fusion | flops 4829184 | bytes 271872 | tf_op jit(solution)/shard_map/hqk,khv->hqv/dot_general | solution.py:117
  8.2 5.6 %all_gather.3 = bf16[96,512]{1,0:T(8,128)(2,1)S(1)} all-gather(bf16[96,256]{1,0:T(8,128)(2,1)S(1)} %bitcast.111), channel_id=1, replica_groups=mesh['sp'=16,'tp'=2] {'tp'}, dimensions={1}, use_global_device_ids=true | all-gather | bytes 147456 | tf_op jit(solution)/shard_map/all_gather | solution.py:144
  13.7 0.0 copy-done
  13.7 0.6 %multiply_reduce_fusion = (f32[96]{0:T(128)S(1)}, f32[96,2048]{1,0:T(8,128)S(1)}) fusion(bf16[96,512]{1,0:T(8,128)(2,1)S(1)} %all_gather.3, bf16[512,2048]{1,0:T(8,128)(2,1)S(1)} %copy-done), kind=kOutput, calls=%fused_computation.25 | convolution fusion | flops 201719712 | bytes 2982272 | tf_op jit(solution)/shard_map/dot_general | solution.py:143
  14.3 0.0 copy-done.7
  14.3 0.9 %multiply_convert_fusion = bf16[96,2048]{1,0:T(8,128)(2,1)} fusion(f32[96,2048]{1,0:T(8,128)S(1)} %get-tuple-element.23, f32[2048]{0:T(1024)S(1)} %copy-done.7, f32[96]{0:T(128)S(1)} %add_rsqrt_fusion), kind=kLoop, calls=%fused_computation.24 | loop fusion | flops 589824 | bytes 1188224 | tf_op jit(solution)/shard_map/convert_element_type | solution.py:148
  (12 shorter events, 0.2 us)
Async XLA Ops:
  0.0 13.7 %copy-start = (bf16[512,2048]{1,0:T(8,128)(2,1)S(1)}, bf16[512,2048]{1,0:T(8,128)(2,1)}, u32[]{:S(2)}) copy-start(bf16[512,2048]{1,0:T(8,128)(2,1)} %param.22) | copy-start | bytes 6291460
  0.0 4.8 %copy-start.1 = (bf16[96,2048]{1,0:T(8,128)(2,1)S(1)}, bf16[96,2048]{1,0:T(8,128)(2,1)}, u32[]{:S(2)}) copy-start(bf16[96,2048]{1,0:T(8,128)(2,1)} %param.12) | copy-start | bytes 1179652
  0.0 4.6 %copy-start.9 = (f32[512]{0:T(512)S(1)}, f32[512]{0:T(512)}, u32[]{:S(2)}) copy-start(f32[512]{0:T(512)} %param.17) | copy-start | bytes 6148
  0.0 4.8 %copy-start.2 = (bf16[2048,512]{1,0:T(8,128)(2,1)S(1)}, bf16[2048,512]{1,0:T(8,128)(2,1)}, u32[]{:S(2)}) copy-start(bf16[2048,512]{1,0:T(8,128)(2,1)} %param.13) | copy-start | bytes 6291460
  1.7 5.5 %collective-permute-start.1 = (bf16[96,64]{0,1:T(8,128)(2,1)S(1)}, bf16[96,64]{0,1:T(8,128)(2,1)S(1)}, u32[]{:S(2)}, u32[]{:S(2)}) collective-permute-start(bf16[96,64]{0,1:T(8,128)(2,1)S(1)} %pad_maximum_fusion.3), channel_id=1, source_target_pairs={{0,2},{2,0},{4,6},{6,4},{8,10},{10,8},{12,14},{14,12},{16,18},{18,... | collective-permute-start | bytes 36872 | tf_op jit(solution)/shard_map/ppermute | solution.py:24
  4.6 1.0 %copy-start.5 = (bf16[512,256]{1,0:T(8,128)(2,1)S(1)}, bf16[512,256]{1,0:T(8,128)(2,1)}, u32[]{:S(2)}) copy-start(bf16[512,256]{1,0:T(8,128)(2,1)} %param.18) | copy-start | bytes 786436
  4.6 1.0 %copy-start.8 = (f32[512]{0:T(512)S(1)}, f32[512]{0:T(512)}, u32[]{:S(2)}) copy-start(f32[512]{0:T(512)} %param.16) | copy-start | bytes 6148
  4.6 1.2 %copy-start.6 = (bf16[512,128]{1,0:T(8,128)(2,1)S(1)}, bf16[512,128]{1,0:T(8,128)(2,1)}, u32[]{:S(2)}) copy-start(bf16[512,128]{1,0:T(8,128)(2,1)} %param.19) | copy-start | bytes 393220
  4.6 1.4 %copy-start.4 = (bf16[512,256]{1,0:T(8,128)(2,1)S(1)}, bf16[512,256]{1,0:T(8,128)(2,1)}, u32[]{:S(2)}) copy-start(bf16[512,256]{1,0:T(8,128)(2,1)} %param.21) | copy-start | bytes 786436
  4.7 1.6 %copy-start.3 = (bf16[512,256]{1,0:T(8,128)(2,1)S(1)}, bf16[512,256]{1,0:T(8,128)(2,1)}, u32[]{:S(2)}) copy-start(bf16[512,256]{1,0:T(8,128)(2,1)} %param.20) | copy-start | bytes 786436
  4.8 2.1 %collective-permute-start = (bf16[96,512]{1,0:T(8,128)(2,1)S(1)}, bf16[96,512]{1,0:T(8,128)(2,1)S(1)}, u32[]{:S(2)}, u32[]{:S(2)}) collective-permute-start(bf16[96,512]{1,0:T(8,128)(2,1)S(1)} %multiply_convert_fusion.1), channel_id=1, source_target_pairs={{0,2},{2,0},{4,6},{6,4},{8,10},{10,8},{12,14},{14,12},{16,18},{18,... | collective-permute-start | bytes 294920 | tf_op jit(solution)/shard_map/ppermute | solution.py:24
  7.7 6.6 %copy-start.7 = (f32[2048]{0:T(1024)S(1)}, f32[2048]{0:T(1024)}, u32[]{:S(2)}) copy-start(f32[2048]{0:T(1024)} %param.23) | copy-start | bytes 24580
where the time goes:
time: 15.4 us; the launch traced here: 15.2 us
  matrix products  7.19 us (47%)
  blocking collectives  5.58 us (36%)
  other arithmetic  1.29 us (8%)
  starting transfers between devices  0.65 us (4%)
  between operations  0.29 us (2%)
  local copies, waits for them, and re-layouts  0.18 us (1%)
    all_gather x1, blocking collectives, on_device(): lax.all_gather(attn_rows, 'tp', axis=1, tiled=True)  5.58 us
    dot_general x1, matrix products, on_device(): jnp.dot(tokens, latent_down, preferred_element_type=jnp.float32)  2.3 us
    dot_general x1, matrix products, on_device(): jnp.dot(tokens, rope_down, preferred_element_type=jnp.float32)  1.48 us
    convert_element_type x1, other arithmetic, on_device(): return normalize(projected, out_gain).astype(jnp.bfloat16)  0.88 us
    ppermute x2, starting transfers between devices, swapped(): return lax.ppermute(value, axis, pairs)  0.65 us
    dot_general x1, matrix products, on_device(): jnp.dot(lax.all_gather(attn_rows, 'tp', axis=1, tiled=True), out_proj, pr...  0.56 us
    dot_general x1, matrix products, on_device(): jnp.dot(tokens, query_down, preferred_element_type=jnp.float32)  0.55 us
    dot_general x2, matrix products, attend(): jnp.einsum('hqk,khv->hqv', expd.astype(jnp.bfloat16), values, preferred_e...  0.44 us
  transfers between devices with their start and end apart: 2, of which 0 were waited for; matrix products, arithmetic and copies ran while one was open for 30% of the time, Pallas kernels for 0%

commit v1 on v0

--- a/solution.py
+++ b/solution.py
@@ -1,7 +1,14 @@
+import functools
+
 import jax
 import jax.numpy as jnp
+import numpy as np
 from jax import lax
+from jax.experimental import pallas as pl
+from jax.experimental.pallas import tpu as pltpu
 from jax.sharding import PartitionSpec as P
+
+MESH = pl.DeviceIdType.MESH
 
 HEADS = 4
 NOPE = 128
@@ -148,6 +155,247 @@
     return normalize(projected, out_gain).astype(jnp.bfloat16)
 
 
+def rotary_tables(length, width):
+    half = ROPE // 2
+    freq = THETA ** (-np.arange(half, dtype=np.float64) / half)
+    angle = np.arange(length, dtype=np.float64)[:, None] * freq[None, :]
+    cosine = np.tile(np.cos(angle), (1, width // half))
+    sine = np.tile(np.concatenate([-np.sin(angle), np.sin(angle)], axis=1), (1, width // ROPE))
+    return cosine.astype(np.float32), sine.astype(np.float32)
+
+
+def fused_kernel(
+    chunks,
+    tok_h, qd_h, ld_h, rd_h, qg_h, lg_h, qu_h, qr_h, ku_h, vu_h, op_h, og_h, cos_h, sin_h,
+    out_h,
+    tok, qd, ld, rd, qg, lg, qu, qr, ku, vu, op, og, cosv, sinv,
+    own, far, attn_own, attn_far, acc,
+    in_sem, qd_sem, ld_sem, send_sem, recv_sem,
+):
+    rows, width = tok.shape
+    latent = ku.shape[0]
+    heads = ku.shape[1] // NOPE
+    sp = lax.axis_index("sp")
+    tp = lax.axis_index("tp")
+    partner = sp + 1 - 2 * lax.rem(sp, 2)
+    across = 1 - tp
+
+    barrier = pltpu.get_barrier_semaphore()
+    pl.semaphore_signal(barrier, inc=1, device_id={"sp": partner}, device_id_type=MESH)
+    pl.semaphore_signal(barrier, inc=1, device_id={"tp": across}, device_id_type=MESH)
+
+    depth = width // chunks
+    mine = pl.ds(pl.multiple_of(lax.rem(sp, 2) * rows, rows), rows)
+    own_rows = pl.ds(pl.multiple_of(tp * heads * VDIM, heads * VDIM), heads * VDIM)
+    far_rows = pl.ds(pl.multiple_of(across * heads * VDIM, heads * VDIM), heads * VDIM)
+
+    def copy(source, target, sem):
+        made = pltpu.make_async_copy(source, target, sem)
+        made.start()
+        return made
+
+    c_tok = copy(tok_h, tok, in_sem.at[0])
+    c_ld = [
+        copy(ld_h.at[pl.ds(k * depth, depth)], ld.at[pl.ds(k * depth, depth)], ld_sem.at[k])
+        for k in range(chunks)
+    ]
+    c_rd = [
+        copy(rd_h, rd.at[pl.ds(h * ROPE, ROPE)], in_sem.at[1 + h]) for h in range(heads)
+    ]
+    c_cos = copy(cos_h.at[mine], cosv, in_sem.at[3])
+    c_sin = copy(sin_h.at[mine], sinv, in_sem.at[4])
+    c_lg = copy(lg_h, lg, in_sem.at[5])
+    c_qd = [
+        copy(qd_h.at[pl.ds(k * depth, depth)], qd.at[pl.ds(k * depth, depth)], qd_sem.at[k])
+        for k in range(chunks)
+    ]
+    c_qg = copy(qg_h, qg, in_sem.at[6])
+    c_qu = copy(qu_h, qu, in_sem.at[7])
+    c_qr = copy(qr_h, qr, in_sem.at[8])
+    c_ku = copy(ku_h, ku, in_sem.at[9])
+    c_vu = copy(vu_h, vu, in_sem.at[10])
+    c_op = [
+        copy(op_h.at[own_rows], op.at[0], in_sem.at[11]),
+        copy(op_h.at[far_rows], op.at[1], in_sem.at[12]),
+    ]
+    c_og = copy(og_h, og, in_sem.at[13])
+
+    def dot(a, b):
+        return jnp.dot(a, b, preferred_element_type=jnp.float32)
+
+    def dot_t(a, b):
+        return lax.dot_general(a, b, (((1,), (1,)), ((), ())), preferred_element_type=jnp.float32)
+
+    def down(weight, copies):
+        total = None
+        for k in range(chunks):
+            copies[k].wait()
+            part = dot(tok[:, k * depth : (k + 1) * depth], weight[k * depth : (k + 1) * depth, :])
+            total = part if total is None else total + part
+        return total
+
+    lane = lax.broadcasted_iota(jnp.int32, (rows, heads * ROPE), 1)
+    low = lane % ROPE < ROPE // 2
+
+    def turned(v):
+        swapped_pair = jnp.where(
+            low,
+            pltpu.roll(v, heads * ROPE - ROPE // 2, 1),
+            pltpu.roll(v, ROPE // 2, 1),
+        )
+        return v * cosv[...] + swapped_pair * sinv[...]
+
+    c_tok.wait()
+    kv = down(ld, c_ld)
+    c_lg.wait()
+    own[:, :latent] = normalize(kv, lg[...]).astype(jnp.bfloat16)
+    for c in c_rd:
+        c.wait()
+    c_cos.wait()
+    c_sin.wait()
+    own[:, latent:] = turned(dot_t(tok[...], rd[...])).astype(jnp.bfloat16)
+
+    pl.semaphore_wait(barrier, 2)
+    kv_send = pltpu.make_async_remote_copy(
+        src_ref=own, dst_ref=far, send_sem=send_sem.at[0], recv_sem=recv_sem.at[0],
+        device_id={"sp": partner}, device_id_type=MESH,
+    )
+    kv_send.start()
+
+    q_sum = down(qd, c_qd)
+    c_qg.wait()
+    q_latent = normalize(q_sum, qg[...]).astype(jnp.bfloat16)
+    c_qu.wait()
+    q_nope = dot(q_latent, qu[...]).astype(jnp.bfloat16)
+    c_qr.wait()
+    q_rot = turned(dot(q_latent, qr[...])).astype(jnp.bfloat16)
+    queries = [
+        jnp.concatenate(
+            [
+                q_nope[:, h * NOPE : (h + 1) * NOPE],
+                jnp.where(lane // ROPE == h, q_rot, jnp.zeros_like(q_rot)),
+            ],
+            axis=1,
+        )
+        for h in range(heads)
+    ]
+    c_ku.wait()
+    c_vu.wait()
+
+    def expand(block):
+        latents = block[:, :latent]
+        rope = block[:, latent:]
+        keys = dot(latents, ku[...]).astype(jnp.bfloat16)
+        values = dot(latents, vu[...]).astype(jnp.bfloat16)
+        scores = [
+            dot_t(queries[h], jnp.concatenate([keys[:, h * NOPE : (h + 1) * NOPE], rope], axis=1))
+            for h in range(heads)
+        ]
+        return scores, values
+
+    scores_own, values_own = expand(own)
+    kv_send.wait_recv()
+    scores_far, values_far = expand(far)
+    scale = (NOPE + ROPE) ** (-0.5)
+    sends = []
+    for h in range(heads):
+        s_own, s_far = scores_own[h], scores_far[h]
+        high = jnp.maximum(
+            jnp.max(s_own, axis=-1, keepdims=True), jnp.max(s_far, axis=-1, keepdims=True)
+        )
+        e_own = jnp.exp((s_own - high) * scale)
+        e_far = jnp.exp((s_far - high) * scale)
+        total = jnp.sum(e_own, axis=-1, keepdims=True) + jnp.sum(e_far, axis=-1, keepdims=True)
+        cols = slice(h * VDIM, (h + 1) * VDIM)
+        weighted = dot(e_own.astype(jnp.bfloat16), values_own[:, cols]) + dot(
+            e_far.astype(jnp.bfloat16), values_far[:, cols]
+        )
+        attn_own[h] = (weighted / total).astype(jnp.bfloat16)
+        send = pltpu.make_async_remote_copy(
+            src_ref=attn_own.at[h], dst_ref=attn_far.at[h],
+            send_sem=send_sem.at[1 + h], recv_sem=recv_sem.at[1 + h],
+            device_id={"tp": across}, device_id_type=MESH,
+        )
+        send.start()
+        sends.append(send)
+
+    c_op[0].wait()
+    held = jnp.concatenate([attn_own[h] for h in range(heads)], axis=1)
+    model = op.shape[2]
+    step = 512
+    for n in range(0, model, step):
+        acc[:, n : n + step] = dot(held, op[0, :, n : n + step])
+    c_op[1].wait()
+    c_og.wait()
+    for send in sends:
+        send.wait_recv()
+    held = jnp.concatenate([attn_far[h] for h in range(heads)], axis=1)
+    squares = jnp.zeros((rows, 1), jnp.float32)
+    for n in range(0, model, step):
+        part = acc[:, n : n + step] + dot(held, op[1, :, n : n + step])
+        acc[:, n : n + step] = part
+        squares = squares + jnp.sum(part * part, axis=-1, keepdims=True)
+    factor = lax.rsqrt(squares / model + EPS)
+    out_h[...] = (acc[...] * factor * og[...]).astype(jnp.bfloat16)
+    kv_send.wait_send()
+    for send in sends:
+        send.wait_send()
+
+
+def fused_on_device(
+    tokens, query_down, latent_down, rope_down, query_gain, latent_gain,
+    query_up, query_rope, key_up, value_up, out_proj, out_gain,
+):
+    rows, width = tokens.shape
+    latent = latent_down.shape[1]
+    heads = key_up.shape[1] // NOPE
+    model = out_proj.shape[1]
+    chunks = 4
+    cosine, sine = rotary_tables(2 * rows, heads * ROPE)
+    bf16, f32 = jnp.bfloat16, jnp.float32
+    args = (
+        tokens, query_down, latent_down, rope_down.T, query_gain[None, :], latent_gain[None, :],
+        query_up, query_rope, key_up, value_up, out_proj, out_gain[None, :],
+        jnp.asarray(cosine), jnp.asarray(sine),
+    )
+    rope_shape = (rows, heads * ROPE)
+    return pl.pallas_call(
+        functools.partial(fused_kernel, chunks),
+        out_shape=pltpu.VMEM((rows, model), bf16),
+        in_specs=[pl.BlockSpec(memory_space=pltpu.HBM)] * len(args),
+        out_specs=pl.BlockSpec(memory_space=pltpu.VMEM),
+        scratch_shapes=[
+            pltpu.VMEM(tokens.shape, bf16),
+            pltpu.VMEM(query_down.shape, bf16),
+            pltpu.VMEM(latent_down.shape, bf16),
+            pltpu.VMEM((heads * ROPE, width), bf16),
+            pltpu.VMEM((1, latent), f32),
+            pltpu.VMEM((1, latent), f32),
+            pltpu.VMEM(query_up.shape, bf16),
+            pltpu.VMEM(query_rope.shape, bf16),
+            pltpu.VMEM(key_up.shape, bf16),
+            pltpu.VMEM(value_up.shape, bf16),
+            pltpu.VMEM((2, heads * VDIM, model), bf16),
+            pltpu.VMEM((1, model), f32),
+            pltpu.VMEM(rope_shape, f32),
+            pltpu.VMEM(rope_shape, f32),
+            pltpu.VMEM((rows, latent + heads * ROPE), bf16),
+            pltpu.VMEM((rows, latent + heads * ROPE), bf16),
+            pltpu.VMEM((heads, rows, VDIM), bf16),
+            pltpu.VMEM((heads, rows, VDIM), bf16),
+            pltpu.VMEM((rows, model), f32),
+            pltpu.SemaphoreType.DMA((14,)),
+            pltpu.SemaphoreType.DMA((chunks,)),
+            pltpu.SemaphoreType.DMA((chunks,)),
+            pltpu.SemaphoreType.DMA((1 + heads,)),
+            pltpu.SemaphoreType.DMA((1 + heads,)),
+        ],
+        compiler_params=pltpu.CompilerParams(
+            collective_id=0, has_side_effects=True, vmem_limit_bytes=67000000 - 2 * rows * model
+        ),
+    )(*args)
+
+
 def solution(mesh):
     in_specs = (
         P("sp", None),
@@ -164,6 +412,8 @@
         P(),
     )
     out_specs = P("sp", None)
+    group = mesh.shape["sp"] // SEQS
+    small = group == 2 and mesh.shape["tp"] == 2 and HEADS // 2 * ROPE == 128
     return jax.shard_map(
-        on_device, mesh=mesh, in_specs=in_specs, out_specs=out_specs, check_vma=False
-    )
+        fused_on_device if small else on_device, mesh=mesh, in_specs=in_specs, out_specs=out_specs, check_vma=False
+    )

time: 15.4 us -> 13 us (0.84)
  Pallas kernels: 0 us -> 12.1 us
  matrix products: 7.19 us -> 0 us
  blocking collectives: 5.58 us -> 0 us
  other arithmetic: 1.29 us -> 0 us
  starting transfers between devices: 0.65 us -> 0 us
  local copies, waits for them, and re-layouts: 0.18 us -> 0.75 us
  between operations: 0.29 us -> 0.01 us
    pallas_call x0 -> x1, Pallas kernels: none -> 12.1 us  [fused_on_device(): pl.pallas_call(functools.partial(fused_kernel, chunks), out_shape=pltpu.V...]
    dot_general x16 -> x0, matrix products: 7.19 us -> none  [the longest x1 2.3 us: on_device(): jnp.dot(tokens, latent_down, preferred_element_type=jnp.float32)]
    all_gather x1 -> x0, blocking collectives: 5.58 us -> none  [on_device(): lax.all_gather(attn_rows, 'tp', axis=1, tiled=True)]
    convert_element_type x3 -> x0, other arithmetic: 0.97 us -> none  [the longest x1 0.88 us: on_device(): return normalize(projected, out_gain).astype(jnp.bfloat16)]
    ppermute x2 -> x0, starting transfers between devices: 0.65 us -> none  [swapped(): return lax.ppermute(value, axis, pairs)]
    unnamed x20 -> x1, local copies, waits for them, and re-layouts: 0.17 us -> 0.75 us
    another operation x2 -> x0, other arithmetic: 0.18 us -> none
  transfers between devices with their start and end apart: 2 -> 0, of which waited for: 0 -> 0; matrix products, arithmetic and copies ran while one was open for 30% -> 0% of each run, Pallas kernels for 0% -> 0%
where the time goes in v1:
time: 13 us; the launch traced here: 12.9 us
  Pallas kernels  12.1 us (93%)
  local copies, waits for them, and re-layouts  0.75 us (6%)
    pallas_call x1, Pallas kernels, fused_on_device(): pl.pallas_call(functools.partial(fused_kernel, chunks), out_shape=pltpu.V...  12.1 us
    unnamed x1, local copies, waits for them, and re-layouts  0.75 us

profile of v1, /device:TPU:0, one launch (start us, length us, event | category | flops | bytes accessed | tf_op | source)
XLA Modules:
  0.0 12.9 jit_solution(12264686872035995525)
XLA Ops:
  0.0 12.1 %shard_map.136 = bf16[96,2048]{1,0:T(8,128)(2,1)S(1)} custom-call(bf16[96,2048]{1,0:T(8,128)(2,1)} %tok_h.1, bf16[2048,512]{1,0:T(8,128)(2,1)} %qd_h.1, bf16[2048,512]{1,0:T(8,128)(2,1)} %ld_h.1, bf16[64,2048]{1,0:T(8,128)(2,1)} %bitcast.4, f32[1,512]{1,0:T(1,128)} %bitcast.6, f32[1,512]{1,0:T(1,128)} %bitcast.7, bf16[512,256]{1,0:T(8,128)(2,1)} %qu_h.1, ...), custom_call_target="tpu_custom_call" | custom-call | tf_op jit(solution)/shard_map/pallas_call | solution.py:362
  12.1 0.7 %copy.16 = bf16[96,2048]{1,0:T(8,128)(2,1)} copy(bf16[96,2048]{1,0:T(8,128)(2,1)S(1)} %shard_map.136) | data formatting | bytes 786432

commit v2 on v1

--- a/solution.py
+++ b/solution.py
@@ -194,45 +194,25 @@
         made.start()
         return made
 
+    def pieces(source, target, sem):
+        return [
+            copy(source.at[pl.ds(k * depth, depth)], target.at[pl.ds(k * depth, depth)], sem.at[k])
+            for k in range(chunks)
+        ]
+
     c_tok = copy(tok_h, tok, in_sem.at[0])
-    c_ld = [
-        copy(ld_h.at[pl.ds(k * depth, depth)], ld.at[pl.ds(k * depth, depth)], ld_sem.at[k])
-        for k in range(chunks)
+    c_rd = copy(rd_h, rd, in_sem.at[1])
+    c_latent = pieces(ld_h, ld, ld_sem) + [
+        copy(lg_h, lg, in_sem.at[4]),
+        copy(cos_h.at[mine], cosv, in_sem.at[2]),
+        copy(sin_h.at[mine], sinv, in_sem.at[3]),
     ]
-    c_rd = [
-        copy(rd_h, rd.at[pl.ds(h * ROPE, ROPE)], in_sem.at[1 + h]) for h in range(heads)
-    ]
-    c_cos = copy(cos_h.at[mine], cosv, in_sem.at[3])
-    c_sin = copy(sin_h.at[mine], sinv, in_sem.at[4])
-    c_lg = copy(lg_h, lg, in_sem.at[5])
-    c_qd = [
-        copy(qd_h.at[pl.ds(k * depth, depth)], qd.at[pl.ds(k * depth, depth)], qd_sem.at[k])
-        for k in range(chunks)
-    ]
-    c_qg = copy(qg_h, qg, in_sem.at[6])
-    c_qu = copy(qu_h, qu, in_sem.at[7])
-    c_qr = copy(qr_h, qr, in_sem.at[8])
-    c_ku = copy(ku_h, ku, in_sem.at[9])
-    c_vu = copy(vu_h, vu, in_sem.at[10])
-    c_op = [
-        copy(op_h.at[own_rows], op.at[0], in_sem.at[11]),
-        copy(op_h.at[far_rows], op.at[1], in_sem.at[12]),
-    ]
-    c_og = copy(og_h, og, in_sem.at[13])
 
     def dot(a, b):
         return jnp.dot(a, b, preferred_element_type=jnp.float32)
 
     def dot_t(a, b):
         return lax.dot_general(a, b, (((1,), (1,)), ((), ())), preferred_element_type=jnp.float32)
-
-    def down(weight, copies):
-        total = None
-        for k in range(chunks):
-            copies[k].wait()
-            part = dot(tok[:, k * depth : (k + 1) * depth], weight[k * depth : (k + 1) * depth, :])
-            total = part if total is None else total + part
-        return total
 
     lane = lax.broadcasted_iota(jnp.int32, (rows, heads * ROPE), 1)
     low = lane % ROPE < ROPE // 2
@@ -245,16 +225,21 @@
         )
         return v * cosv[...] + swapped_pair * sinv[...]
 
+    pl.delay(150)
+    c_expand = [copy(ku_h, ku, in_sem.at[8]), copy(vu_h, vu, in_sem.at[9])]
+    c_query = pieces(qd_h, qd, qd_sem) + [
+        copy(qg_h, qg, in_sem.at[5]),
+        copy(qu_h, qu, in_sem.at[6]),
+        copy(qr_h, qr, in_sem.at[7]),
+    ]
     c_tok.wait()
-    kv = down(ld, c_ld)
-    c_lg.wait()
+    c_rd.wait()
+    rope_raw = dot_t(tok[...], jnp.concatenate([rd[...]] * heads, axis=0))
+    for c in c_latent:
+        c.wait()
+    kv = dot(tok[...], ld[...])
+    own[:, latent:] = turned(rope_raw).astype(jnp.bfloat16)
     own[:, :latent] = normalize(kv, lg[...]).astype(jnp.bfloat16)
-    for c in c_rd:
-        c.wait()
-    c_cos.wait()
-    c_sin.wait()
-    own[:, latent:] = turned(dot_t(tok[...], rd[...])).astype(jnp.bfloat16)
-
     pl.semaphore_wait(barrier, 2)
     kv_send = pltpu.make_async_remote_copy(
         src_ref=own, dst_ref=far, send_sem=send_sem.at[0], recv_sem=recv_sem.at[0],
@@ -262,13 +247,27 @@
     )
     kv_send.start()
 
-    q_sum = down(qd, c_qd)
-    c_qg.wait()
-    q_latent = normalize(q_sum, qg[...]).astype(jnp.bfloat16)
-    c_qu.wait()
-    q_nope = dot(q_latent, qu[...]).astype(jnp.bfloat16)
-    c_qr.wait()
-    q_rot = turned(dot(q_latent, qr[...])).astype(jnp.bfloat16)
+    def expand(block):
+        latents = block[:, :latent]
+        keys = dot(latents, ku[...]).astype(jnp.bfloat16)
+        values = dot(latents, vu[...]).astype(jnp.bfloat16)
+        return keys, block[:, latent:], values
+
+    c_out = [
+        copy(op_h.at[own_rows], op.at[0], in_sem.at[10]),
+        copy(op_h.at[far_rows], op.at[1], in_sem.at[11]),
+        copy(og_h, og, in_sem.at[12]),
+    ]
+    for c in c_expand:
+        c.wait()
+    held_own = expand(own)
+    for c in c_query:
+        c.wait()
+    q_raw = dot(tok[...], qd[...])
+    q_factor = lax.rsqrt(jnp.mean(q_raw * q_raw, axis=-1, keepdims=True) + EPS)
+    q_gained = (q_raw * qg[...]).astype(jnp.bfloat16)
+    q_nope = (dot(q_gained, qu[...]) * q_factor).astype(jnp.bfloat16)
+    q_rot = (turned(dot(q_gained, qr[...])) * q_factor).astype(jnp.bfloat16)
     queries = [
         jnp.concatenate(
             [
@@ -279,27 +278,18 @@
         )
         for h in range(heads)
     ]
-    c_ku.wait()
-    c_vu.wait()
-
-    def expand(block):
-        latents = block[:, :latent]
-        rope = block[:, latent:]
-        keys = dot(latents, ku[...]).astype(jnp.bfloat16)
-        values = dot(latents, vu[...]).astype(jnp.bfloat16)
-        scores = [
-            dot_t(queries[h], jnp.concatenate([keys[:, h * NOPE : (h + 1) * NOPE], rope], axis=1))
-            for h in range(heads)
-        ]
-        return scores, values
-
-    scores_own, values_own = expand(own)
+    def score(held, h):
+        keys, rope, _ = held
+        full = jnp.concatenate([keys[:, h * NOPE : (h + 1) * NOPE], rope], axis=1)
+        return dot_t(queries[h], full)
+
     kv_send.wait_recv()
-    scores_far, values_far = expand(far)
+    held_far = expand(far)
+    scores_own = [score(held_own, h) for h in range(heads)]
     scale = (NOPE + ROPE) ** (-0.5)
     sends = []
     for h in range(heads):
-        s_own, s_far = scores_own[h], scores_far[h]
+        s_own, s_far = scores_own[h], score(held_far, h)
         high = jnp.maximum(
             jnp.max(s_own, axis=-1, keepdims=True), jnp.max(s_far, axis=-1, keepdims=True)
         )
@@ -307,8 +297,8 @@
         e_far = jnp.exp((s_far - high) * scale)
         total = jnp.sum(e_own, axis=-1, keepdims=True) + jnp.sum(e_far, axis=-1, keepdims=True)
         cols = slice(h * VDIM, (h + 1) * VDIM)
-        weighted = dot(e_own.astype(jnp.bfloat16), values_own[:, cols]) + dot(
-            e_far.astype(jnp.bfloat16), values_far[:, cols]
+        weighted = dot(e_own.astype(jnp.bfloat16), held_own[2][:, cols]) + dot(
+            e_far.astype(jnp.bfloat16), held_far[2][:, cols]
         )
         attn_own[h] = (weighted / total).astype(jnp.bfloat16)
         send = pltpu.make_async_remote_copy(
@@ -319,14 +309,13 @@
         send.start()
         sends.append(send)
 
-    c_op[0].wait()
+    for c in c_out:
+        c.wait()
     held = jnp.concatenate([attn_own[h] for h in range(heads)], axis=1)
     model = op.shape[2]
     step = 512
     for n in range(0, model, step):
         acc[:, n : n + step] = dot(held, op[0, :, n : n + step])
-    c_op[1].wait()
-    c_og.wait()
     for send in sends:
         send.wait_recv()
     held = jnp.concatenate([attn_far[h] for h in range(heads)], axis=1)
@@ -368,7 +357,7 @@
             pltpu.VMEM(tokens.shape, bf16),
             pltpu.VMEM(query_down.shape, bf16),
             pltpu.VMEM(latent_down.shape, bf16),
-            pltpu.VMEM((heads * ROPE, width), bf16),
+            pltpu.VMEM((ROPE, width), bf16),
             pltpu.VMEM((1, latent), f32),
             pltpu.VMEM((1, latent), f32),
             pltpu.VMEM(query_up.shape, bf16),

time: 13 us -> 10.7 us (0.82)
  Pallas kernels: 12.1 us -> 9.81 us
    pallas_call x1, Pallas kernels: 12.1 us -> 9.81 us  [fused_on_device(): pl.pallas_call(functools.partial(fused_kernel, chunks), out_shape=pltpu.V...]
where the time goes in v2:
time: 10.7 us; the launch traced here: 10.6 us
  Pallas kernels  9.81 us (92%)
  local copies, waits for them, and re-layouts  0.75 us (7%)
    pallas_call x1, Pallas kernels, fused_on_device(): pl.pallas_call(functools.partial(fused_kernel, chunks), out_shape=pltpu.V...  9.81 us
    unnamed x1, local copies, waits for them, and re-layouts  0.75 us

profile of v2, /device:TPU:0, one launch (start us, length us, event | category | flops | bytes accessed | tf_op | source)
XLA Modules:
  0.0 10.6 jit_solution(10876899289865526249)
XLA Ops:
  0.0 9.8 %shard_map.136 = bf16[96,2048]{1,0:T(8,128)(2,1)S(1)} custom-call(bf16[96,2048]{1,0:T(8,128)(2,1)} %tok_h.1, bf16[2048,512]{1,0:T(8,128)(2,1)} %qd_h.1, bf16[2048,512]{1,0:T(8,128)(2,1)} %ld_h.1, bf16[64,2048]{1,0:T(8,128)(2,1)} %bitcast.4, f32[1,512]{1,0:T(1,128)} %bitcast.6, f32[1,512]{1,0:T(1,128)} %bitcast.7, bf16[512,256]{1,0:T(8,128)(2,1)} %qu_h.1, ...), custom_call_target="tpu_custom_call" | custom-call | tf_op jit(solution)/shard_map/pallas_call | solution.py:351
  9.8 0.7 %copy.16 = bf16[96,2048]{1,0:T(8,128)(2,1)} copy(bf16[96,2048]{1,0:T(8,128)(2,1)S(1)} %shard_map.136) | data formatting | bytes 786432

commit v3 on v2

--- a/solution.py
+++ b/solution.py
@@ -290,12 +290,10 @@
     sends = []
     for h in range(heads):
         s_own, s_far = scores_own[h], score(held_far, h)
-        high = jnp.maximum(
-            jnp.max(s_own, axis=-1, keepdims=True), jnp.max(s_far, axis=-1, keepdims=True)
-        )
+        high = jnp.max(jnp.maximum(s_own, s_far), axis=-1, keepdims=True)
         e_own = jnp.exp((s_own - high) * scale)
         e_far = jnp.exp((s_far - high) * scale)
-        total = jnp.sum(e_own, axis=-1, keepdims=True) + jnp.sum(e_far, axis=-1, keepdims=True)
+        total = jnp.sum(e_own + e_far, axis=-1, keepdims=True)
         cols = slice(h * VDIM, (h + 1) * VDIM)
         weighted = dot(e_own.astype(jnp.bfloat16), held_own[2][:, cols]) + dot(
             e_far.astype(jnp.bfloat16), held_far[2][:, cols]

time: 10.7 us -> 10.7 us (level)
  no operation moved by 1% of the time
where the time goes in v3:
time: 10.7 us; the launch traced here: 10.6 us
  Pallas kernels  9.81 us (92%)
  local copies, waits for them, and re-layouts  0.75 us (7%)
    pallas_call x1, Pallas kernels, fused_on_device(): pl.pallas_call(functools.partial(fused_kernel, chunks), out_shape=pltpu.V...  9.81 us
    unnamed x1, local copies, waits for them, and re-layouts  0.75 us

profile of v3, /device:TPU:0, one launch (start us, length us, event | category | flops | bytes accessed | tf_op | source)
XLA Modules:
  0.0 10.6 jit_solution(9993754842415700145)
XLA Ops:
  0.0 9.8 %shard_map.136 = bf16[96,2048]{1,0:T(8,128)(2,1)S(1)} custom-call(bf16[96,2048]{1,0:T(8,128)(2,1)} %tok_h.1, bf16[2048,512]{1,0:T(8,128)(2,1)} %qd_h.1, bf16[2048,512]{1,0:T(8,128)(2,1)} %ld_h.1, bf16[64,2048]{1,0:T(8,128)(2,1)} %bitcast.4, f32[1,512]{1,0:T(1,128)} %bitcast.6, f32[1,512]{1,0:T(1,128)} %bitcast.7, bf16[512,256]{1,0:T(8,128)(2,1)} %qu_h.1, ...), custom_call_target="tpu_custom_call" | custom-call | tf_op jit(solution)/shard_map/pallas_call | solution.py:349
  9.8 0.7 %copy.16 = bf16[96,2048]{1,0:T(8,128)(2,1)} copy(bf16[96,2048]{1,0:T(8,128)(2,1)S(1)} %shard_map.136) | data formatting | bytes 786432
